TPU v7x, 32 devices: a whole 2x2x4 slice. The times are simulated.
32 devices in a mesh: ep: 8 (over z, y), tp: 4 (over x, core).
Axes of the slice: x: 2, y: 2, z: 4, core: 2. Of those that a mesh axis runs over, the one named last changes fastest.
Arguments:
- mixer_input: bfloat16 [4096, 2048], P('ep'), may hold values from -6 to 6
- log_forget_total: float32 [16, 4096], P('tp'), may hold values from -684 to 0, as said below
- mixer_gain: float32 [2048], replicated, may hold values from 0.1 to 1.9
- w_query: bfloat16 [2048, 1024], P(None, 'tp'), may hold values from -1 to 1
- w_key: bfloat16 [2048, 256], P(None, 'tp'), may hold values from -8 to 8
- w_value: bfloat16 [2048, 256], P(None, 'tp'), may hold values from -0.125 to 0.125
- w_output: bfloat16 [1024, 2048], replicated, may hold values from -0.1875 to 0.1875
- mixer_post_gain: float32 [2048], replicated, may hold values from 0.1 to 1.9
- expert_input: bfloat16 [2048, 2048], P('ep'), may hold values from -6 to 6
- expert_ids: int32 [2048, 2], P('ep'), may hold values from 0 to 7, all different within a row; in each aligned block of 64 rows (0 to 63, 64 to 127, ...) at most 32 rows name the same one
- route_weight: float32 [2048, 2], P('ep'), may hold values from 0.1 to 1
- expert_gain: float32 [2048], replicated, may hold values from 0.1 to 1.9
- w_gate: bfloat16 [8, 2048, 3584], P('ep', None, 'tp'), may hold values from -0.125 to 0.125
- w_up: bfloat16 [8, 2048, 3584], P('ep', None, 'tp'), may hold values from -0.125 to 0.125
- w_down: bfloat16 [8, 3584, 2048], P('ep', 'tp'), may hold values from -0.09375 to 0.09375
- expert_post_gain: float32 [2048], replicated, may hold values from 0.1 to 1.9
Outputs:
- mixer_out: bfloat16 [4096, 2048], P(('ep', 'tp'))
- expert_out: bfloat16 [2048, 2048], P(('ep', 'tp'))
Inputs may be any that keep to these rules, and one draw needn't show every extreme that they name: `expert_ids`: in each aligned block of 64 tokens no expert is named by more than 32 of them. `log_forget_total`: each head's values never rise along the positions.
All inputs are finite; a program needn't handle non-finite values.
Results may differ from a plain program's by a relative error of at most 0.012.
The roundings to bfloat16 on the way count: a program that leaves them out, or rounds other values in their place, can miss the bound.
Values may be sent and summed in bfloat16 or wider, within the bound.
A program may use at most 128 MiB of HBM per device.

v0:
```python
import math
import jax
import jax.numpy as jnp
from jax import lax
from jax.sharding import PartitionSpec as P

HD = 64
TOP_K = 2
NEG_FILL = -1e30
NORM_EPS = 1e-06


def norm_rows(values_in, gain_vec):
    widened = values_in.astype(jnp.float32)
    return (
        widened
        * lax.rsqrt(jnp.mean(widened * widened, axis=-1, keepdims=True) + NORM_EPS)
        * gain_vec
    )


def unchanged(present_state):
    return present_state


def mixer_half(
    mixer_input, log_forget_total, mixer_gain, w_query, w_key, w_value, w_output, mixer_post_gain
):
    row_count = mixer_input.shape[0]
    offset = lax.axis_index("ep") * row_count
    head_local = w_query.shape[1] // HD
    kv_local = w_key.shape[1] // HD
    group_size = head_local // kv_local
    normed = norm_rows(mixer_input, mixer_gain).astype(jnp.bfloat16)
    queries = (
        jnp.dot(normed, w_query, preferred_element_type=jnp.float32)
        .astype(jnp.bfloat16)
        .reshape(row_count, kv_local, group_size, HD)
    )
    key_rows = (
        jnp.dot(normed, w_key, preferred_element_type=jnp.float32)
        .astype(jnp.bfloat16)
        .reshape(row_count, kv_local, HD)
    )
    value_rows = (
        jnp.dot(normed, w_value, preferred_element_type=jnp.float32)
        .astype(jnp.bfloat16)
        .reshape(row_count, kv_local, HD)
    )
    gate_totals = log_forget_total.reshape(kv_local, group_size, -1)
    query_gate = lax.dynamic_slice_in_dim(gate_totals, offset, row_count, 2)
    query_pos = offset + jnp.arange(row_count, dtype=jnp.int32)
    last_row = offset + row_count - 1
    score_scale = HD ** (-0.5)
    start_state = (
        jnp.full((kv_local, group_size, row_count), NEG_FILL, jnp.float32),
        jnp.zeros((kv_local, group_size, row_count), jnp.float32),
        jnp.zeros((kv_local, group_size, row_count, HD), jnp.float32),
    )
    running = start_state
    key_piece = lax.all_gather(key_rows, "ep", axis=0, tiled=True)
    value_piece = lax.all_gather(value_rows, "ep", axis=0, tiled=True)
    piece_rows = key_piece.shape[0]
    block_rows = math.gcd(piece_rows, 512)
    block_total = piece_rows // block_rows
    key_blocks = key_piece.reshape(block_total, block_rows, kv_local, HD)
    value_blocks = value_piece.reshape(block_total, block_rows, kv_local, HD)

    def one_block(present_state, operands):
        key_block, value_block, block_index = operands
        block_first = block_index * block_rows

        def update(prior_value):
            row_max, denominator, numerator = prior_value
            key_gate = lax.dynamic_slice_in_dim(gate_totals, block_first, block_rows, 2)
            scores = (
                jnp.einsum("qgjd,kgd->gjqk", queries, key_block, preferred_element_type=jnp.float32)
                * score_scale
            )
            scores = scores + query_gate[:, :, :, None] - key_gate[:, :, None, :]
            visible = (block_first + jnp.arange(block_rows, dtype=jnp.int32))[None, :] <= query_pos[
                :, None
            ]
            scores = jnp.where(visible, scores, NEG_FILL)
            new_max = jnp.maximum(row_max, jnp.max(scores, axis=-1))
            shifted = jnp.where(visible, jnp.exp(scores - new_max[..., None]), 0.0)
            factor = jnp.exp(row_max - new_max)
            denominator = denominator * factor + jnp.sum(shifted, axis=-1)
            numerator = numerator * factor[..., None] + jnp.einsum(
                "gjqk,kgd->gjqd",
                shifted.astype(jnp.bfloat16),
                value_block,
                preferred_element_type=jnp.float32,
            )
            return (new_max, denominator, numerator)

        return (lax.cond(block_first <= last_row, update, unchanged, present_state), None)

    running, _ = lax.scan(
        one_block, running, (key_blocks, value_blocks, jnp.arange(block_total, dtype=jnp.int32))
    )
    row_max, denominator, numerator = running
    mixed_heads = (
        jnp.transpose(numerator / denominator[..., None], (2, 0, 1, 3))
        .reshape(row_count, head_local * HD)
        .astype(jnp.bfloat16)
    )
    by_rows = lax.all_to_all(mixed_heads, "tp", split_axis=0, concat_axis=1, tiled=True)
    projected = jnp.dot(by_rows, w_output, preferred_element_type=jnp.float32)
    return norm_rows(projected, mixer_post_gain).astype(jnp.bfloat16)


def expert_half(
    expert_input, expert_ids, route_weight, expert_gain, w_gate, w_up, w_down, expert_post_gain
):
    row_count = expert_input.shape[0]
    quarters = lax.axis_size("tp")
    experts = lax.axis_size("ep")
    quarter_rows = row_count // quarters
    slot_count = 2 * TOP_K * quarter_rows // experts
    own_quarter = lax.axis_index("tp")
    normed = norm_rows(expert_input, expert_gain).astype(jnp.bfloat16)
    padded_rows = jnp.concatenate([normed, jnp.zeros((1, normed.shape[1]), jnp.bfloat16)], axis=0)
    routed = expert_ids.reshape(quarters, quarter_rows * TOP_K)
    matches = (routed[:, :, None] == jnp.arange(experts, dtype=jnp.int32)[None, None, :]).astype(
        jnp.int32
    )
    slot_ranks = jnp.sum(jnp.cumsum(matches, axis=1) * matches, axis=2) - 1
    owners = (jnp.arange(row_count * TOP_K, dtype=jnp.int32) // TOP_K).reshape(
        quarters, quarter_rows * TOP_K
    )
    quarter_index = jnp.broadcast_to(jnp.arange(quarters, dtype=jnp.int32)[:, None], routed.shape)
    slot_table = (
        jnp.full((quarters, slot_count, experts), row_count, jnp.int32)
        .at[quarter_index, slot_ranks, routed]
        .set(owners)
    )
    gate_local = w_gate[0]
    up_local = w_up[0]
    down_local = w_down[0]
    unit_count = gate_local.shape[1]
    own_table = lax.dynamic_index_in_dim(slot_table, own_quarter, 0, keepdims=False)
    outgoing = padded_rows[own_table]
    arrived = lax.all_to_all(outgoing, "ep", split_axis=1, concat_axis=1, tiled=True)
    slot_rows = lax.all_gather(arrived[None], "tp", axis=0, tiled=True)
    flat_rows = slot_rows.reshape(-1, slot_rows.shape[-1])
    gate_part = jnp.dot(flat_rows, gate_local, preferred_element_type=jnp.float32)
    up_part = jnp.dot(flat_rows, up_local, preferred_element_type=jnp.float32)
    hidden = (
        (jax.nn.silu(gate_part) * up_part)
        .astype(jnp.bfloat16)
        .reshape(slot_rows.shape[:-1] + (unit_count,))
    )
    product = jnp.dot(
        hidden.reshape(-1, unit_count), down_local, preferred_element_type=jnp.float32
    )
    summed = lax.psum_scatter(
        product.reshape(lax.axis_size("tp") * 1, slot_count, experts, product.shape[-1]).astype(
            jnp.bfloat16
        ),
        "tp",
        scatter_dimension=0,
        tiled=True,
    ).astype(jnp.float32)
    results = summed[0].astype(jnp.bfloat16)
    returned = lax.all_to_all(results, "ep", split_axis=1, concat_axis=1, tiled=True)
    flat_results = returned.reshape(slot_count * experts, returned.shape[-1])
    own_routes = lax.dynamic_index_in_dim(routed, own_quarter, 0, keepdims=False)
    own_ranks = lax.dynamic_index_in_dim(slot_ranks, own_quarter, 0, keepdims=False)
    picked = flat_results[own_ranks * experts + own_routes].reshape(quarter_rows, TOP_K, -1)
    own_weights = lax.dynamic_slice_in_dim(
        route_weight, own_quarter * quarter_rows, quarter_rows, 0
    )
    combined = jnp.sum(own_weights[:, :, None] * picked.astype(jnp.float32), axis=1)
    return norm_rows(combined, expert_post_gain).astype(jnp.bfloat16)


def per_device(
    mixer_input,
    log_forget_total,
    mixer_gain,
    w_query,
    w_key,
    w_value,
    w_output,
    mixer_post_gain,
    expert_input,
    expert_ids,
    route_weight,
    expert_gain,
    w_gate,
    w_up,
    w_down,
    expert_post_gain,
):
    mixer_out = mixer_half(
        mixer_input,
        log_forget_total,
        mixer_gain,
        w_query,
        w_key,
        w_value,
        w_output,
        mixer_post_gain,
    )
    expert_out = expert_half(
        expert_input, expert_ids, route_weight, expert_gain, w_gate, w_up, w_down, expert_post_gain
    )
    return (mixer_out, expert_out)


def solution(mesh):
    placed = (
        P("ep", None),
        P("tp", None),
        P(),
        P(None, "tp"),
        P(None, "tp"),
        P(None, "tp"),
        P(),
        P(),
        P("ep", None),
        P("ep", None),
        P("ep", None),
        P(),
        P("ep", None, "tp"),
        P("ep", None, "tp"),
        P("ep", "tp", None),
        P(),
    )
    return jax.shard_map(
        per_device,
        mesh=mesh,
        in_specs=placed,
        out_specs=(P(("ep", "tp"), None), P(("ep", "tp"), None)),
        check_vma=False,
    )
```

profile of v0, /device:TPU:0, one launch (start us, length us, event | category | flops | bytes accessed | tf_op | source)
XLA Modules:
  0.0 324.2 jit_solution(3863174267052389493)
XLA Ops:
  7.2 0.9 copy.41
  9.2 29.5 %scatter_fusion = s32[4,32,8]{1,2,0:T(8,128)S(1)} fusion(s32[4,32,8]{1,2,0:T(8,128)S(1)} %broadcast_in_dim.39, s32[512]{0:T(512)S(1)} %fusion.52, s32[512]{0:T(512)S(1)} %fusion.54), kind=kCustom, calls=%fused_computation.2 | custom fusion | bytes 12288 | tf_op jit(solution)/shard_map/scatter | solution.py:136
  39.7 1.4 gather_fusion
  41.0 0.6 copy.44
  41.6 32.9 %all_to_all.26 = bf16[32,8,2048]{2,0,1:T(8,128)(2,1)S(1)} all-to-all(bf16[32,8,2048]{2,0,1:T(8,128)(2,1)S(1)} %copy.44), channel_id=1, replica_groups=mesh['ep'=8,'tp'=4] {'ep'}, dimensions={1} | all-to-all | bytes 2097152 | tf_op jit(solution)/shard_map/all_to_all | solution.py:144
  74.5 1.6 copy.45
  76.3 33.4 %all-gather.5.cloned.1.call-done = bf16[128,8,2048]{2,1,0:T(8,128)(2,1)} async-done(((bf16[32,8,2048]{2,1,0:T(8,128)(2,1)}), bf16[128,8,2048]{2,1,0:T(8,128)(2,1)}) %all-gather.5.cloned.1.call-update) | async-done | bytes 4194320 | tf_op jit(solution)/shard_map/all_gather | solution.py:145
  109.7 7.5 %fusion.32 = f32[1024,896]{1,0:T(8,128)S(1)} fusion(bf16[128,8,2048]{2,1,0:T(8,128)(2,1)} %all-gather.5.cloned.1.call-done, bf16[1,2048,896]{2,1,0:T(8,128)(2,1)} %param.33), kind=kOutput, calls=%fused_computation.40 | convolution fusion | flops 3758096384 | bytes 11534336 | tf_op jit(solution)/shard_map/dot_general | solution.py:148
  117.2 4.8 %multiply_convert_fusion = bf16[1024,896]{1,0:T(8,128)(2,1)S(1)} fusion(f32[1024,896]{1,0:T(8,128)S(1)} %fusion.32, bf16[1,2048,896]{2,1,0:T(8,128)(2,1)S(1)} %copy-done.11, bf16[128,8,2048]{2,1,0:T(8,128)(2,1)S(1)} %copy-done.10), kind=kOutput, calls=%fused_computation.48 | convolution fusion | flops 3763601408 | bytes 13369344 | tf_op jit(solution)/shard_map/dot_general | solution.py:147
  122.0 6.0 %convolution_convert_fusion = bf16[4,32,8,2048]{3,2,1,0:T(8,128)(2,1)} fusion(bf16[4,32,8,896]{3,2,1,0:T(8,128)(2,1)S(1)} %bitcast.163, bf16[1,896,2048]{2,1,0:T(8,128)(2,1)S(1)} %copy-done.12), kind=kOutput, calls=%fused_computation.44 | convolution fusion | flops 3760193536 | bytes 9699328 | tf_op jit(solution)/shard_map/dot_general | solution.py:154
  128.0 1.5 copy-done.1
  129.6 0.5 fusion.29
  130.1 2.2 fusion.31
  132.3 0.8 convolution_convert_fusion.3
  133.0 31.5 %all-gather = bf16[4096,64]{0,1:T(8,128)(2,1)S(1)} all-gather(bf16[512,64]{0,1:T(8,128)(2,1)S(1)} %convolution_convert_fusion.3), channel_id=2, replica_groups=mesh['ep'=8,'tp'=4] {'ep'}, dimensions={0}, use_global_device_ids=true | all-gather | bytes 589824 | tf_op jit(solution)/shard_map/all_gather | solution.py:61
  164.7 0.9 copy.37
  165.6 0.8 convolution_convert_fusion.2
  166.4 31.4 %all-gather.1 = bf16[4096,64]{0,1:T(8,128)(2,1)S(1)} all-gather(bf16[512,64]{0,1:T(8,128)(2,1)S(1)} %convolution_convert_fusion.2), channel_id=3, replica_groups=mesh['ep'=8,'tp'=4] {'ep'}, dimensions={0}, use_global_device_ids=true | all-gather | bytes 589824 | tf_op jit(solution)/shard_map/all_gather | solution.py:62
  198.0 1.0 copy.38
  199.0 0.7 dynamic-slice_bitcast_fusion.1
  199.7 1.5 convolution_convert_fusion.1
  201.2 18.1 %while.15 = (s32[]{:T(128)}, f32[1,4,512]{2,1,0:T(4,128)S(1)}, f32[1,4,512]{2,1,0:T(4,128)S(1)}, f32[1,4,512,64]{2,3,1,0:T(8,128)S(1)}, s32[8]{0:T(128)S(1)}, /*...) while((s32[]{:T(128)}, f32[1,4,512]{2,1,0:T(4,128)S(1)}, ...), condition=%wide.region_6.7_spmd.clone, body=%wide.region_1.6_spmd.clone.sunk | while | flops 288889856 | bytes 15283569 | solution.py:99
  201.2 0.7 dynamic_slice.79
  202.5 7.4 %conditional.3 = ((f32[1,4,512]{2,1,0:T(4,128)S(1)}, f32[1,4,512]{2,1,0:T(4,128)S(1)}, f32[1,4,512,64]{2,3,1,0:T(8,128)S(1)})) conditional(s32[]{:T(128)} %convert_element_type.123, (f32[1,4,512]{2,1,0:T(4,128)S(1)}, f32[1,4,512]{2,1,0:T(4,128)S(1)}, f32[1,4,512,64]{2,3,1,0:T(8,128)S(1)}) %tuple.48, (s32[]{:T(128)}, s32[]{:T(128)}, ...), branch_computations={%region_2.2_spmd, %region_3.5_spmd} | conditional | flops 288889856 | bytes 15281230 | solution.py:97
  202.5 0.8 dynamic-slice_bitcast_fusion
  203.6 2.2 fusion.6
  205.8 2.6 fusion.14
  208.4 1.5 fusion.5
  210.0 0.7 dynamic_slice.79
  211.3 0.7 dynamic_slice.79
  212.6 0.7 dynamic_slice.79
  214.0 0.7 dynamic_slice.79
  215.3 0.7 dynamic_slice.79
  216.7 0.7 dynamic_slice.79
  218.0 0.7 dynamic_slice.79
  219.5 0.7 copy.39
  220.2 3.4 %all-to-all-start = ((bf16[4,128,256]{1,2,0:T(8,128)(2,1)}), bf16[4,128,256]{1,2,0:T(8,128)(2,1)S(1)}, u32[]{:S(2)}, u32[]{:S(2)}) async-start(bf16[4,128,256]{1,2,0:T(8,128)(2,1)} %copy.39), calls=%async_computation | async-start | bytes 524288 | tf_op jit(solution)/shard_map/all_to_all | solution.py:108
  223.7 2.8 copy.46
  226.5 3.1 all-to-all-done
  229.6 57.5 %all-to-all-start.2 = ((bf16[32,8,2048]{2,0,1:T(8,128)(2,1)}), bf16[32,8,2048]{2,0,1:T(8,128)(2,1)S(1)}, u32[]{:S(2)}, u32[]{:S(2)}) async-start(bf16[32,8,2048]{2,0,1:T(8,128)(2,1)} %copy.46), calls=%async_computation.3 | async-start | bytes 2097152 | tf_op jit(solution)/shard_map/all_to_all | solution.py:166
  287.3 3.0 multiply_reduce_fusion.1
  290.3 1.0 multiply_convert_fusion.1
  291.3 21.4 %all-to-all-done.2 = bf16[32,8,2048]{2,0,1:T(8,128)(2,1)S(1)} async-done(((bf16[32,8,2048]{2,0,1:T(8,128)(2,1)}), bf16[32,8,2048]{2,0,1:T(8,128)(2,1)S(1)}, u32[]{:S(2)}, u32[]{:S(2)}) %all-to-all-start.2) | async-done | bytes 1048608 | tf_op jit(solution)/shard_map/all_to_all | solution.py:166
  312.7 0.6 copy.53
  313.3 0.9 gather_fusion.1
  314.2 0.7 reshape.287
  314.9 1.5 multiply_reduce_fusion
  316.6 0.8 multiply_convert_fusion.2
  (83 shorter events, 3.4 us)
Async XLA Ops:
  7.2 192.5 %copy-start = (bf16[2048,256]{1,0:T(8,128)(2,1)S(1)}, bf16[2048,256]{1,0:T(8,128)(2,1)}, u32[]{:S(2)}) copy-start(bf16[2048,256]{1,0:T(8,128)(2,1)} %param.23) | copy-start | bytes 3145732
  7.2 31.8 %copy-start.2 = (bf16[256,2048]{1,0:T(8,128)(2,1)S(1)}, bf16[256,2048]{1,0:T(8,128)(2,1)}, u32[]{:S(2)}) copy-start(bf16[256,2048]{1,0:T(8,128)(2,1)} %param.28) | copy-start | bytes 3145732
  7.2 32.1 %copy-start.5 = (f32[2048]{0:T(1024)S(1)}, f32[2048]{0:T(1024)}, u32[]{:S(2)}) copy-start(f32[2048]{0:T(1024)} %param.31) | copy-start | bytes 24580
  7.2 102.5 %all-gather.5.cloned.1.call-start = ((), (), s32[]{:S(2)}) async-start(), calls=%async_computation.5 | async-start | bytes 5242880 | tf_op jit(solution)/shard_map/all_gather | solution.py:145
  76.1 147.6 %reduce-scatter.2.cloned.1.call-start = ((), (), s32[]{:S(2)}) async-start(), calls=%async_computation.4 | async-start | bytes 5242880 | tf_op jit(solution)/shard_map/reduce_scatter | solution.py:157
  109.7 7.5 %copy-start.10 = (bf16[128,8,2048]{2,1,0:T(8,128)(2,1)S(1)}, bf16[128,8,2048]{2,1,0:T(8,128)(2,1)}, u32[]{:S(2)}) copy-start(bf16[128,8,2048]{2,1,0:T(8,128)(2,1)} %all-gather.5.cloned.1.call-done) | copy-start | bytes 12582916
  109.7 7.5 %copy-start.11 = (bf16[1,2048,896]{2,1,0:T(8,128)(2,1)S(1)}, bf16[1,2048,896]{2,1,0:T(8,128)(2,1)}, u32[]{:S(2)}) copy-start(bf16[1,2048,896]{2,1,0:T(8,128)(2,1)} %param.32) | copy-start | bytes 11010052
  117.2 4.8 %copy-start.12 = (bf16[1,896,2048]{2,1,0:T(8,128)(2,1)S(1)}, bf16[1,896,2048]{2,1,0:T(8,128)(2,1)}, u32[]{:S(2)}) copy-start(bf16[1,896,2048]{2,1,0:T(8,128)(2,1)} %param.34) | copy-start | bytes 11010052
  128.0 1.6 copy-start.1
  128.0 2.1 copy-start.6
  128.0 4.3 %copy-start.3 = (bf16[2048,64]{0,1:T(8,128)(2,1)S(1)}, bf16[2048,64]{0,1:T(8,128)(2,1)}, u32[]{:S(2)}) copy-start(bf16[2048,64]{0,1:T(8,128)(2,1)} %param.24) | copy-start | bytes 786436
  130.1 35.5 %copy-start.4 = (bf16[2048,64]{0,1:T(8,128)(2,1)S(1)}, bf16[2048,64]{0,1:T(8,128)(2,1)}, u32[]{:S(2)}) copy-start(bf16[2048,64]{0,1:T(8,128)(2,1)} %param.25) | copy-start | bytes 786436
  219.4 67.7 %copy-start.9 = (f32[256,2]{0,1:T(2,128)S(1)}, f32[256,2]{0,1:T(2,128)}, u32[]{:S(2)}) copy-start(f32[256,2]{0,1:T(2,128)} %param.30) | copy-start | bytes 6148
  220.2 9.4 %all-to-all-start = ((bf16[4,128,256]{1,2,0:T(8,128)(2,1)}), bf16[4,128,256]{1,2,0:T(8,128)(2,1)S(1)}, u32[]{:S(2)}, u32[]{:S(2)}) async-start(bf16[4,128,256]{1,2,0:T(8,128)(2,1)} %copy.39), calls=%async_computation | async-start | bytes 524288 | tf_op jit(solution)/shard_map/all_to_all | solution.py:108
  226.5 63.9 %copy-start.7 = (f32[2048]{0:T(1024)S(1)}, f32[2048]{0:T(1024)}, u32[]{:S(2)}) copy-start(f32[2048]{0:T(1024)} %param.27) | copy-start | bytes 24580
  229.6 83.1 %all-to-all-start.2 = ((bf16[32,8,2048]{2,0,1:T(8,128)(2,1)}), bf16[32,8,2048]{2,0,1:T(8,128)(2,1)S(1)}, u32[]{:S(2)}, u32[]{:S(2)}) async-start(bf16[32,8,2048]{2,0,1:T(8,128)(2,1)} %copy.46), calls=%async_computation.3 | async-start | bytes 2097152 | tf_op jit(solution)/shard_map/all_to_all | solution.py:166
  313.3 3.3 %copy-start.8 = (f32[2048]{0:T(1024)S(1)}, f32[2048]{0:T(1024)}, u32[]{:S(2)}) copy-start(f32[2048]{0:T(1024)} %param.35) | copy-start | bytes 24580
Sparse Core Ops, SparseCore 0:
  76.2 33.4 all-gather.4
  128.1 44.5 reduce-scatter.1
where the time goes:
time: 326 us; the launch traced here: 324 us
  blocking collectives  95.8 us (29%)
  starting transfers between devices  61.1 us (19%)
  waiting for transfers between devices  58 us (18%)
  local copies, waits for them, and re-layouts  51.1 us (16%)
  matrix products  29 us (9%)
  between operations  14.4 us (4%)
  other arithmetic  9.24 us (3%)
  loops' own time  5.57 us (2%)
    all_to_all x1, starting transfers between devices, expert_half(): lax.all_to_all(results, 'ep', split_axis=1, concat_axis=1, tiled=True)  57.5 us
    all_gather x1, waiting for transfers between devices, expert_half(): slot_rows = lax.all_gather(arrived[None], 'tp', axis=0, tiled=True)  33.4 us
    all_to_all x1, blocking collectives, expert_half(): lax.all_to_all(outgoing, 'ep', split_axis=1, concat_axis=1, tiled=True)  32.9 us
    all_gather x1, blocking collectives, mixer_half(): key_piece = lax.all_gather(key_rows, 'ep', axis=0, tiled=True)  31.5 us
    all_gather x1, blocking collectives, mixer_half(): value_piece = lax.all_gather(value_rows, 'ep', axis=0, tiled=True)  31.4 us
    scatter x1, local copies, waits for them, and re-layouts, expert_half(): slot_table = jnp.full((quarters, slot_count, experts), row_count, jnp.int...  29.5 us
    all_to_all x1, waiting for transfers between devices, expert_half(): lax.all_to_all(results, 'ep', split_axis=1, concat_axis=1, tiled=True)  21.4 us
    dot_general x1, matrix products, expert_half(): up_part = jnp.dot(flat_rows, up_local, preferred_element_type=jnp.float32)  7.49 us
  transfers between devices with their start and end apart: 4, of which 3 were waited for; matrix products, arithmetic and copies ran while one was open for 9% of the time, Pallas kernels for 0%

commit v1 on v0

--- a/solution.py
+++ b/solution.py
@@ -58,7 +58,12 @@
         jnp.zeros((kv_local, group_size, row_count, HD), jnp.float32),
     )
     running = start_state
-    key_piece = lax.all_gather(key_rows, "ep", axis=0, tiled=True)
+    ring = [key_rows]
+    for hop in range(7):
+        ring.append(lax.ppermute(ring[-1], "ep", [(dev, (dev + 1) % 8) for dev in range(8)]))
+    key_piece = jnp.roll(
+        jnp.concatenate(ring[::-1], axis=0), (lax.axis_index("ep") + 1) * ring[0].shape[0], axis=0
+    )
     value_piece = lax.all_gather(value_rows, "ep", axis=0, tiled=True)
     piece_rows = key_piece.shape[0]
     block_rows = math.gcd(piece_rows, 512)

time: 326 us -> 313 us (0.960)
  waiting for transfers between devices: 58 us -> 94.5 us
  blocking collectives: 95.8 us -> 64.5 us
  starting transfers between devices: 61.1 us -> 49.3 us
    ppermute x0 -> x7, waiting for transfers between devices: none -> 36.5 us  [mixer_half(): lax.ppermute(ring[-1], 'ep', [(dev, (dev + 1) % 8) for dev in range(8)])]
    all_gather x1 -> x0, blocking collectives: 31.5 us -> none  [mixer_half(): key_piece = lax.all_gather(key_rows, 'ep', axis=0, tiled=True)]
    all_to_all x1, starting transfers between devices: 57.5 us -> 42 us  [expert_half(): lax.all_to_all(results, 'ep', split_axis=1, concat_axis=1, tiled=True)]
    ppermute x0 -> x7, starting transfers between devices: none -> 3.64 us  [mixer_half(): lax.ppermute(ring[-1], 'ep', [(dev, (dev + 1) % 8) for dev in range(8)])]
  transfers between devices with their start and end apart: 4 -> 11, of which waited for: 3 -> 9; matrix products, arithmetic and copies ran while one was open for 9% -> 7% of each run, Pallas kernels for 0% -> 0%
where the time goes in v1:
time: 313 us; the launch traced here: 312 us
  waiting for transfers between devices  94.5 us (30%)
  blocking collectives  64.5 us (21%)
  local copies, waits for them, and re-layouts  49.5 us (16%)
  starting transfers between devices  49.3 us (16%)
  matrix products  26.5 us (8%)
  between operations  14.6 us (5%)
  other arithmetic  7.61 us (2%)
  loops' own time  6.04 us (2%)
    all_to_all x1, starting transfers between devices, expert_half(): lax.all_to_all(results, 'ep', split_axis=1, concat_axis=1, tiled=True)  42 us
    ppermute x7, waiting for transfers between devices, mixer_half(): lax.ppermute(ring[-1], 'ep', [(dev, (dev + 1) % 8) for dev in range(8)])  36.5 us
    all_gather x1, waiting for transfers between devices, expert_half(): slot_rows = lax.all_gather(arrived[None], 'tp', axis=0, tiled=True)  33.4 us
    all_to_all x1, blocking collectives, expert_half(): lax.all_to_all(outgoing, 'ep', split_axis=1, concat_axis=1, tiled=True)  32.9 us
    all_gather x1, blocking collectives, mixer_half(): value_piece = lax.all_gather(value_rows, 'ep', axis=0, tiled=True)  31.6 us
    scatter x1, local copies, waits for them, and re-layouts, expert_half(): slot_table = jnp.full((quarters, slot_count, experts), row_count, jnp.int...  29.5 us
    all_to_all x1, waiting for transfers between devices, expert_half(): lax.all_to_all(results, 'ep', split_axis=1, concat_axis=1, tiled=True)  21.4 us
    dot_general x1, matrix products, expert_half(): up_part = jnp.dot(flat_rows, up_local, preferred_element_type=jnp.float32)  7.49 us
  transfers between devices with their start and end apart: 11, of which 9 were waited for; matrix products, arithmetic and copies ran while one was open for 7% of the time, Pallas kernels for 0%

profile of v1, /device:TPU:0, one launch (start us, length us, event | category | flops | bytes accessed | tf_op | source)
XLA Modules:
  0.0 312.4 jit_solution(12251461355318069971)
XLA Ops:
  7.2 0.9 copy.40
  9.2 29.5 %scatter_fusion = s32[4,32,8]{1,2,0:T(8,128)S(1)} fusion(s32[4,32,8]{1,2,0:T(8,128)S(1)} %broadcast_in_dim.39, s32[512]{0:T(512)S(1)} %fusion.53, s32[512]{0:T(512)S(1)} %fusion.55), kind=kCustom, calls=%fused_computation.2 | custom fusion | bytes 12288 | tf_op jit(solution)/shard_map/scatter | solution.py:141
  39.7 1.4 gather_fusion
  41.6 32.9 %all_to_all.26 = bf16[32,8,2048]{2,0,1:T(8,128)(2,1)S(1)} all-to-all(bf16[32,8,2048]{2,0,1:T(8,128)(2,1)S(1)} %copy.43), channel_id=1, replica_groups=mesh['ep'=8,'tp'=4] {'ep'}, dimensions={1} | all-to-all | bytes 2097152 | tf_op jit(solution)/shard_map/all_to_all | solution.py:149
  74.5 1.6 copy.44
  76.3 33.4 %all-gather.4.cloned.1.call-done = bf16[128,8,2048]{2,1,0:T(8,128)(2,1)} async-done(((bf16[32,8,2048]{2,1,0:T(8,128)(2,1)}), bf16[128,8,2048]{2,1,0:T(8,128)(2,1)}) %all-gather.4.cloned.1.call-update) | async-done | bytes 4194320 | tf_op jit(solution)/shard_map/all_gather | solution.py:150
  109.7 7.5 %fusion.32 = f32[1024,896]{1,0:T(8,128)S(1)} fusion(bf16[128,8,2048]{2,1,0:T(8,128)(2,1)} %all-gather.4.cloned.1.call-done, bf16[1,2048,896]{2,1,0:T(8,128)(2,1)} %param.33), kind=kOutput, calls=%fused_computation.40 | convolution fusion | flops 3758096384 | bytes 11534336 | tf_op jit(solution)/shard_map/dot_general | solution.py:153
  117.2 4.7 %multiply_convert_fusion = bf16[1024,896]{1,0:T(8,128)(2,1)S(1)} fusion(f32[1024,896]{1,0:T(8,128)S(1)} %fusion.32, bf16[1,2048,896]{2,1,0:T(8,128)(2,1)S(1)} %copy-done.11, bf16[128,8,2048]{2,1,0:T(8,128)(2,1)S(1)} %copy-done.10), kind=kOutput, calls=%fused_computation.48 | convolution fusion | flops 3763601408 | bytes 13369344 | tf_op jit(solution)/shard_map/dot_general | solution.py:152
  122.0 6.0 %convolution_convert_fusion = bf16[4,32,8,2048]{3,2,1,0:T(8,128)(2,1)} fusion(bf16[4,32,8,896]{3,2,1,0:T(8,128)(2,1)S(1)} %bitcast.164, bf16[1,896,2048]{2,1,0:T(8,128)(2,1)S(1)} %copy-done.12), kind=kOutput, calls=%fused_computation.44 | convolution fusion | flops 3760193536 | bytes 9699328 | tf_op jit(solution)/shard_map/dot_general | solution.py:159
  128.0 1.6 copy-done.1
  130.7 0.8 fusion.46
  131.4 1.5 collective-permute-start
  132.9 5.5 %collective-permute-done = bf16[512,1,64]{0,2,1:T(8,128)(2,1)S(1)} collective-permute-done((bf16[512,1,64]{0,2,1:T(8,128)(2,1)S(1)}, bf16[512,1,64]{0,2,1:T(8,128)(2,1)S(1)}, u32[]{:S(2)}, u32[]{:S(2)}) %collective-permute-start) | collective-permute-done | bytes 65568 | tf_op jit(solution)/shard_map/ppermute | solution.py:63
  138.4 7.0 %collective-permute-done.1 = bf16[512,1,64]{0,2,1:T(8,128)(2,1)S(1)} collective-permute-done((bf16[512,1,64]{0,2,1:T(8,128)(2,1)S(1)}, bf16[512,1,64]{0,2,1:T(8,128)(2,1)S(1)}, u32[]{:S(2)}, u32[]{:S(2)}) %collective-permute-start.1) | collective-permute-done | bytes 65568 | tf_op jit(solution)/shard_map/ppermute | solution.py:63
  145.4 7.0 %collective-permute-done.2 = bf16[512,1,64]{0,2,1:T(8,128)(2,1)S(1)} collective-permute-done((bf16[512,1,64]{0,2,1:T(8,128)(2,1)S(1)}, bf16[512,1,64]{0,2,1:T(8,128)(2,1)S(1)}, u32[]{:S(2)}, u32[]{:S(2)}) %collective-permute-start.2) | collective-permute-done | bytes 65568 | tf_op jit(solution)/shard_map/ppermute | solution.py:63
  152.4 0.8 convolution_convert_fusion.1
  153.1 6.2 %collective-permute-done.3 = bf16[512,1,64]{0,2,1:T(8,128)(2,1)S(1)} collective-permute-done((bf16[512,1,64]{0,2,1:T(8,128)(2,1)S(1)}, bf16[512,1,64]{0,2,1:T(8,128)(2,1)S(1)}, u32[]{:S(2)}, u32[]{:S(2)}) %collective-permute-start.3) | collective-permute-done | bytes 65568 | tf_op jit(solution)/shard_map/ppermute | solution.py:63
  159.3 0.8 convolution_convert_fusion.2
  160.1 6.4 %collective-permute-done.4 = bf16[512,1,64]{0,2,1:T(8,128)(2,1)S(1)} collective-permute-done((bf16[512,1,64]{0,2,1:T(8,128)(2,1)S(1)}, bf16[512,1,64]{0,2,1:T(8,128)(2,1)S(1)}, u32[]{:S(2)}, u32[]{:S(2)}) %collective-permute-start.4) | collective-permute-done | bytes 65568 | tf_op jit(solution)/shard_map/ppermute | solution.py:63
  166.5 31.6 %all-gather = bf16[4096,64]{0,1:T(8,128)(2,1)S(1)} all-gather(bf16[512,64]{0,1:T(8,128)(2,1)S(1)} %convolution_convert_fusion.2), channel_id=2, replica_groups=mesh['ep'=8,'tp'=4] {'ep'}, dimensions={0}, use_global_device_ids=true | all-gather | bytes 589824 | tf_op jit(solution)/shard_map/all_gather | solution.py:67
  198.5 2.1 collective-permute-start.6
  200.6 0.7 dynamic-slice_bitcast_fusion.1
  201.3 4.4 %collective-permute-done.6 = bf16[512,1,64]{0,2,1:T(8,128)(2,1)S(1)} collective-permute-done((bf16[512,1,64]{0,2,1:T(8,128)(2,1)S(1)}, bf16[512,1,64]{0,2,1:T(8,128)(2,1)S(1)}, u32[]{:S(2)}, u32[]{:S(2)}) %collective-permute-start.6) | collective-permute-done | bytes 65568 | tf_op jit(solution)/shard_map/ppermute | solution.py:63
  206.1 16.9 %while.15 = (s32[]{:T(128)}, f32[1,4,512]{2,1,0:T(4,128)S(1)}, f32[1,4,512]{2,1,0:T(4,128)S(1)}, f32[1,4,512,64]{2,3,1,0:T(8,128)S(1)}, s32[8]{0:T(128)S(1)}, /*...) while((s32[]{:T(128)}, f32[1,4,512]{2,1,0:T(4,128)S(1)}, ...), condition=%wide.region_6.7_spmd.clone, body=%wide.region_1.6_spmd.clone.sunk | while | flops 288889856 | bytes 15282553 | solution.py:104
  206.1 0.7 dynamic_slice.85
  207.5 5.6 %conditional.3 = ((f32[1,4,512]{2,1,0:T(4,128)S(1)}, f32[1,4,512]{2,1,0:T(4,128)S(1)}, f32[1,4,512,64]{2,3,1,0:T(8,128)S(1)})) conditional(s32[]{:T(128)} %convert_element_type.125, (f32[1,4,512]{2,1,0:T(4,128)S(1)}, f32[1,4,512]{2,1,0:T(4,128)S(1)}, f32[1,4,512,64]{2,3,1,0:T(8,128)S(1)}) %tuple.48, (s32[]{:T(128)}, s32[]{:T(128)}, ...), branch_computations={%region_2.2_spmd, %region_3.5_spmd} | conditional | flops 288889856 | bytes 15280214 | solution.py:102
  207.5 0.8 dynamic-slice_bitcast_fusion
  208.6 1.2 fusion.6
  209.8 1.7 fusion.14
  211.5 1.5 fusion.5
  213.1 0.7 dynamic_slice.85
  214.5 0.7 dynamic_slice.85
  215.9 0.7 dynamic_slice.85
  217.4 0.7 dynamic_slice.85
  218.8 0.7 dynamic_slice.85
  220.2 0.7 dynamic_slice.85
  221.6 0.7 dynamic_slice.85
  223.2 0.7 copy.38
  223.9 3.4 %all-to-all-start = ((bf16[4,128,256]{1,2,0:T(8,128)(2,1)}), bf16[4,128,256]{1,2,0:T(8,128)(2,1)S(1)}, u32[]{:S(2)}, u32[]{:S(2)}) async-start(bf16[4,128,256]{1,2,0:T(8,128)(2,1)} %copy.38), calls=%async_computation | async-start | bytes 524288 | tf_op jit(solution)/shard_map/all_to_all | solution.py:113
  227.4 2.8 copy.45
  230.1 3.2 %all-to-all-done = bf16[4,128,256]{1,2,0:T(8,128)(2,1)S(1)} async-done(((bf16[4,128,256]{1,2,0:T(8,128)(2,1)}), bf16[4,128,256]{1,2,0:T(8,128)(2,1)S(1)}, u32[]{:S(2)}, u32[]{:S(2)}) %all-to-all-start) | async-done | bytes 262176 | tf_op jit(solution)/shard_map/all_to_all | solution.py:113
  233.3 42.0 %all-to-all-start.2 = ((bf16[32,8,2048]{2,0,1:T(8,128)(2,1)}), bf16[32,8,2048]{2,0,1:T(8,128)(2,1)S(1)}, u32[]{:S(2)}, u32[]{:S(2)}) async-start(bf16[32,8,2048]{2,0,1:T(8,128)(2,1)} %copy.45), calls=%async_computation.3 | async-start | bytes 2097152 | tf_op jit(solution)/shard_map/all_to_all | solution.py:171
  275.5 3.0 multiply_reduce_fusion.1
  278.5 1.0 multiply_convert_fusion.1
  279.5 21.4 %all-to-all-done.2 = bf16[32,8,2048]{2,0,1:T(8,128)(2,1)S(1)} async-done(((bf16[32,8,2048]{2,0,1:T(8,128)(2,1)}), bf16[32,8,2048]{2,0,1:T(8,128)(2,1)S(1)}, u32[]{:S(2)}, u32[]{:S(2)}) %all-to-all-start.2) | async-done | bytes 1048608 | tf_op jit(solution)/shard_map/all_to_all | solution.py:171
  301.5 0.9 gather_fusion.1
  303.0 1.5 multiply_reduce_fusion
  304.7 0.8 multiply_convert_fusion.2
  (112 shorter events, 6.4 us)
Async XLA Ops:
  7.2 145.2 %copy-start = (bf16[2048,256]{1,0:T(8,128)(2,1)S(1)}, bf16[2048,256]{1,0:T(8,128)(2,1)}, u32[]{:S(2)}) copy-start(bf16[2048,256]{1,0:T(8,128)(2,1)} %param.23) | copy-start | bytes 3145732
  7.2 31.8 %copy-start.2 = (bf16[256,2048]{1,0:T(8,128)(2,1)S(1)}, bf16[256,2048]{1,0:T(8,128)(2,1)}, u32[]{:S(2)}) copy-start(bf16[256,2048]{1,0:T(8,128)(2,1)} %param.28) | copy-start | bytes 3145732
  7.2 32.1 %copy-start.5 = (f32[2048]{0:T(1024)S(1)}, f32[2048]{0:T(1024)}, u32[]{:S(2)}) copy-start(f32[2048]{0:T(1024)} %param.31) | copy-start | bytes 24580
  7.2 102.5 %all-gather.4.cloned.1.call-start = ((), (), s32[]{:S(2)}) async-start(), calls=%async_computation.5 | async-start | bytes 5242880 | tf_op jit(solution)/shard_map/all_gather | solution.py:150
  76.1 151.3 %reduce-scatter.2.cloned.1.call-start = ((), (), s32[]{:S(2)}) async-start(), calls=%async_computation.4 | async-start | bytes 5242880 | tf_op jit(solution)/shard_map/reduce_scatter | solution.py:162
  109.7 7.5 %copy-start.10 = (bf16[128,8,2048]{2,1,0:T(8,128)(2,1)S(1)}, bf16[128,8,2048]{2,1,0:T(8,128)(2,1)}, u32[]{:S(2)}) copy-start(bf16[128,8,2048]{2,1,0:T(8,128)(2,1)} %all-gather.4.cloned.1.call-done) | copy-start | bytes 12582916
  109.7 7.5 %copy-start.11 = (bf16[1,2048,896]{2,1,0:T(8,128)(2,1)S(1)}, bf16[1,2048,896]{2,1,0:T(8,128)(2,1)}, u32[]{:S(2)}) copy-start(bf16[1,2048,896]{2,1,0:T(8,128)(2,1)} %param.32) | copy-start | bytes 11010052
  117.2 4.8 %copy-start.12 = (bf16[1,896,2048]{2,1,0:T(8,128)(2,1)S(1)}, bf16[1,896,2048]{2,1,0:T(8,128)(2,1)}, u32[]{:S(2)}) copy-start(bf16[1,896,2048]{2,1,0:T(8,128)(2,1)} %param.34) | copy-start | bytes 11010052
  128.0 1.6 copy-start.1
  128.0 2.1 copy-start.6
  129.6 1.1 copy-start.3
  130.1 29.2 %copy-start.4 = (bf16[2048,64]{0,1:T(8,128)(2,1)S(1)}, bf16[2048,64]{0,1:T(8,128)(2,1)}, u32[]{:S(2)}) copy-start(bf16[2048,64]{0,1:T(8,128)(2,1)} %param.25) | copy-start | bytes 786436
  131.4 7.0 %collective-permute-start = (bf16[512,1,64]{0,2,1:T(8,128)(2,1)S(1)}, bf16[512,1,64]{0,2,1:T(8,128)(2,1)S(1)}, u32[]{:S(2)}, u32[]{:S(2)}) collective-permute-start(bf16[512,1,64]{0,2,1:T(8,128)(2,1)S(1)} %fusion.46), channel_id=1, source_target_pairs={{0,4},{4,8},{8,12},{12,16},{16,20},{20,24},{24,28},{28,0},{1,5},{5... | collective-permute-start | bytes 196616 | tf_op jit(solution)/shard_map/ppermute | solution.py:63
  138.4 7.0 %collective-permute-start.1 = (bf16[512,1,64]{0,2,1:T(8,128)(2,1)S(1)}, bf16[512,1,64]{0,2,1:T(8,128)(2,1)S(1)}, u32[]{:S(2)}, u32[]{:S(2)}) collective-permute-start(bf16[512,1,64]{0,2,1:T(8,128)(2,1)S(1)} %collective-permute-done), channel_id=1, source_target_pairs={{0,4},{4,8},{8,12},{12,16},{16,20},{20,24},{24,28},{28,0},{1,5},{5... | collective-permute-start | bytes 196616 | tf_op jit(solution)/shard_map/ppermute | solution.py:63
  145.4 7.0 %collective-permute-start.2 = (bf16[512,1,64]{0,2,1:T(8,128)(2,1)S(1)}, bf16[512,1,64]{0,2,1:T(8,128)(2,1)S(1)}, u32[]{:S(2)}, u32[]{:S(2)}) collective-permute-start(bf16[512,1,64]{0,2,1:T(8,128)(2,1)S(1)} %collective-permute-done.1), channel_id=1, source_target_pairs={{0,4},{4,8},{8,12},{12,16},{16,20},{20,24},{24,28},{28,0},{1,5},{5... | collective-permute-start | bytes 196616 | tf_op jit(solution)/shard_map/ppermute | solution.py:63
  152.4 7.0 %collective-permute-start.3 = (bf16[512,1,64]{0,2,1:T(8,128)(2,1)S(1)}, bf16[512,1,64]{0,2,1:T(8,128)(2,1)S(1)}, u32[]{:S(2)}, u32[]{:S(2)}) collective-permute-start(bf16[512,1,64]{0,2,1:T(8,128)(2,1)S(1)} %collective-permute-done.2), channel_id=1, source_target_pairs={{0,4},{4,8},{8,12},{12,16},{16,20},{20,24},{24,28},{28,0},{1,5},{5... | collective-permute-start | bytes 196616 | tf_op jit(solution)/shard_map/ppermute | solution.py:63
  159.3 7.2 %collective-permute-start.4 = (bf16[512,1,64]{0,2,1:T(8,128)(2,1)S(1)}, bf16[512,1,64]{0,2,1:T(8,128)(2,1)S(1)}, u32[]{:S(2)}, u32[]{:S(2)}) collective-permute-start(bf16[512,1,64]{0,2,1:T(8,128)(2,1)S(1)} %collective-permute-done.3), channel_id=1, source_target_pairs={{0,4},{4,8},{8,12},{12,16},{16,20},{20,24},{24,28},{28,0},{1,5},{5... | collective-permute-start | bytes 196616 | tf_op jit(solution)/shard_map/ppermute | solution.py:63
  166.5 32.0 %collective-permute-start.5 = (bf16[512,1,64]{0,2,1:T(8,128)(2,1)S(1)}, bf16[512,1,64]{0,2,1:T(8,128)(2,1)S(1)}, u32[]{:S(2)}, u32[]{:S(2)}) collective-permute-start(bf16[512,1,64]{0,2,1:T(8,128)(2,1)S(1)} %collective-permute-done.4), channel_id=1, source_target_pairs={{0,4},{4,8},{8,12},{12,16},{16,20},{20,24},{24,28},{28,0},{1,5},{5... | collective-permute-start | bytes 196616 | tf_op jit(solution)/shard_map/ppermute | solution.py:63
  198.5 7.2 %collective-permute-start.6 = (bf16[512,1,64]{0,2,1:T(8,128)(2,1)S(1)}, bf16[512,1,64]{0,2,1:T(8,128)(2,1)S(1)}, u32[]{:S(2)}, u32[]{:S(2)}) collective-permute-start(bf16[512,1,64]{0,2,1:T(8,128)(2,1)S(1)} %collective-permute-done.5), channel_id=1, source_target_pairs={{0,4},{4,8},{8,12},{12,16},{16,20},{20,24},{24,28},{28,0},{1,5},{5... | collective-permute-start | bytes 196616 | tf_op jit(solution)/shard_map/ppermute | solution.py:63
  223.0 52.2 %copy-start.9 = (f32[256,2]{0,1:T(2,128)S(1)}, f32[256,2]{0,1:T(2,128)}, u32[]{:S(2)}) copy-start(f32[256,2]{0,1:T(2,128)} %param.30) | copy-start | bytes 6148
  223.9 9.4 %all-to-all-start = ((bf16[4,128,256]{1,2,0:T(8,128)(2,1)}), bf16[4,128,256]{1,2,0:T(8,128)(2,1)S(1)}, u32[]{:S(2)}, u32[]{:S(2)}) async-start(bf16[4,128,256]{1,2,0:T(8,128)(2,1)} %copy.38), calls=%async_computation | async-start | bytes 524288 | tf_op jit(solution)/shard_map/all_to_all | solution.py:113
  230.1 48.4 %copy-start.7 = (f32[2048]{0:T(1024)S(1)}, f32[2048]{0:T(1024)}, u32[]{:S(2)}) copy-start(f32[2048]{0:T(1024)} %param.27) | copy-start | bytes 24580
  233.3 67.6 %all-to-all-start.2 = ((bf16[32,8,2048]{2,0,1:T(8,128)(2,1)}), bf16[32,8,2048]{2,0,1:T(8,128)(2,1)S(1)}, u32[]{:S(2)}, u32[]{:S(2)}) async-start(bf16[32,8,2048]{2,0,1:T(8,128)(2,1)} %copy.45), calls=%async_computation.3 | async-start | bytes 2097152 | tf_op jit(solution)/shard_map/all_to_all | solution.py:171
  301.4 3.3 %copy-start.8 = (f32[2048]{0:T(1024)S(1)}, f32[2048]{0:T(1024)}, u32[]{:S(2)}) copy-start(f32[2048]{0:T(1024)} %param.35) | copy-start | bytes 24580
Sparse Core Ops, SparseCore 0:
  76.2 33.4 all-gather.3
  128.1 44.5 reduce-scatter.1
